TPU v7x, 512 devices: a whole 4x4x16 slice. The times are simulated.
512 devices in a mesh: sp: 32 (over z, core), tp: 16 (over y, x).
Axes of the slice: x: 4, y: 4, z: 16, core: 2. Of those that a mesh axis runs over, the one named last changes fastest.
Arguments:
- prompt: bfloat16 [32, 8192, 2048], P('tp', 'sp'), may hold values from -6 to 6
- input_gain: float32 [2048], replicated, may hold values from 0.1 to 1.9
- key_weight: bfloat16 [1024, 2048], P('tp'), may hold values from -0.125 to 0.125
- value_weight: bfloat16 [1024, 2048], P('tp'), may hold values from -0.125 to 0.125
- key_gain: float32 [64], replicated, may hold values from 0.1 to 1.9
- queries: bfloat16 [32, 2, 1024], P('sp', None, 'tp'), may hold values from -6 to 6
- score_bias: float32 [2, 16], replicated, may hold values from -9 to -2
Outputs:
- keys: bfloat16 [32, 1024, 8192], P('sp', 'tp')
- values: bfloat16 [32, 1024, 8192], P('sp', 'tp')
- first_read: bfloat16 [32, 2, 1024], P('sp', None, 'tp')
All inputs are finite; a program needn't handle non-finite values.
Results may differ from a plain program's by a relative error of at most 0.01.
Values may be sent and summed in bfloat16 or wider, within the bound.
A program may use at most 64 MiB of HBM per device.

v0:
```python
import math

import jax
import jax.numpy as jnp
from jax import lax
from jax.sharding import PartitionSpec as P

HEAD = 64


epsilon = 1e-06


def local(prompt, input_gain, key_weight, value_weight, key_gain, queries, score_bias):
    seq_here, pos_here, width = prompt.shape
    flat = prompt.astype(jnp.float32)
    normed = (
        flat * lax.rsqrt(jnp.mean(flat * flat, axis=-1, keepdims=True) + epsilon) * input_gain
    ).astype(jnp.bfloat16)
    stacked = jnp.stack([key_weight, value_weight])
    columns = key_weight.shape[0]
    kv_width = columns * lax.axis_size("tp")
    projected = jnp.einsum(
        "spd,knd->sknp",
        normed,
        lax.all_gather(stacked, "tp", axis=1, tiled=True),
        preferred_element_type=jnp.float32,
    )
    key_raw = projected[:, 0].reshape(seq_here, kv_width // HEAD, HEAD, pos_here)
    key_norm = (
        key_raw
        * lax.rsqrt(jnp.mean(key_raw * key_raw, axis=2, keepdims=True) + epsilon)
        * key_gain[:, None]
    )
    key_rows = key_norm.reshape(seq_here, kv_width, pos_here).astype(jnp.bfloat16)
    value_rows = projected[:, 1].astype(jnp.bfloat16)
    packed = jnp.stack([key_rows, value_rows], axis=1)
    by_sequence = lax.all_to_all(
        lax.all_to_all(packed, "tp", split_axis=2, concat_axis=0, tiled=True),
        "sp",
        split_axis=0,
        concat_axis=3,
        tiled=True,
    )
    keys = by_sequence[:, 0]
    values = by_sequence[:, 1]
    length = keys.shape[2]
    group = queries.shape[1]
    heads_here = columns // HEAD
    query_heads = queries[0].reshape(group, heads_here, HEAD)
    cache_keys = keys[0].reshape(heads_here, HEAD, length)
    scores = jnp.einsum("ghd,hds->ghs", query_heads, cache_keys, preferred_element_type=jnp.float32)
    first_head = lax.axis_index("tp") * heads_here
    offsets = lax.dynamic_slice_in_dim(score_bias, first_head, heads_here, 1)
    scores = scores / math.sqrt(HEAD) + offsets[:, :, None]
    log_break = jax.nn.log_sigmoid(scores)
    log_keep = jax.nn.log_sigmoid(-scores)
    later = lax.cumsum(log_keep, axis=2, reverse=True) - log_keep
    weights = jnp.exp(log_break + later).astype(jnp.bfloat16)
    cache_values = values[0].reshape(heads_here, HEAD, length)
    first_read = jnp.einsum(
        "ghs,hds->ghd", weights, cache_values, preferred_element_type=jnp.float32
    )
    first_read = first_read.astype(jnp.bfloat16).reshape(1, group, columns)
    return (keys, values, first_read)


def solution(mesh):
    placed = (P("tp", "sp", None), P(), P("tp", None), P("tp", None), P(), P("sp", None, "tp"), P())
    return jax.shard_map(
        local,
        mesh=mesh,
        in_specs=placed,
        out_specs=(P("sp", "tp", None), P("sp", "tp", None), P("sp", None, "tp")),
        check_vma=False,
    )
```

profile of v0, /device:TPU:1, one launch (start us, length us, event | category | flops | bytes accessed | tf_op | source)
XLA Modules:
  0.0 279.9 jit_solution(15170525460887294352)
XLA Ops:
  7.2 0.0 copy-start
  7.2 0.0 copy-start.4
  7.2 0.0 copy-start.5
  7.2 0.0 all-gather.2.cloned.1.call-start
  7.2 2.0 pad_maximum_fusion.1
  9.3 0.0 all-gather.2.cloned.1.call-update
  9.3 0.7 mul.65
  9.9 0.1 mul.66
  10.0 2.1 fusion.5
  12.1 90.8 %all-gather.2.cloned.1.call-done = bf16[2,1024,2048]{2,1,0:T(8,128)(2,1)} async-done(((bf16[2,64,2048]{2,1,0:T(8,128)(2,1)}), bf16[2,1024,2048]{2,1,0:T(8,128)(2,1)}) %all-gather.2.cloned.1.call-update) | async-done | bytes 8388624 | tf_op jit(solution)/shard_map/all_gather | solution.py:26
  102.9 0.0 copy-done.4
  102.9 0.0 copy-done.5
  102.9 7.1 %fusion.8 = f32[2,2,1024,256]{3,2,0,1:T(8,128)S(1)} fusion(bf16[2,1024,2048]{2,1,0:T(8,128)(2,1)} %all-gather.2.cloned.1.call-done, bf16[2,256,2048]{2,1,0:T(8,128)(2,1)S(1)} %copy-done.4, f32[2048]{0:T(1024)S(1)} %copy-done.5, f32[2,256]{1,0:T(2,128)S(1)} %add_rsqrt_fusion.1), kind=kOutput, calls=%fused_computation.11 | convolution fusion | flops 4299161600 | bytes 14690304 | tf_op jit(solution)/shard_map/spd,knd->sknp/dot_general | solution.py:23
  110.0 0.0 copy-start.3
  110.0 0.1 slice_multiply_fusion
  110.2 1.8 copy-done.3
  111.9 0.1 slice.45
  112.0 0.2 reduce_sum.19
  112.3 1.9 fusion.14
  114.2 0.2 pad_maximum_fusion
  114.4 2.2 copy.23
  116.5 32.2 %all_to_all.36 = bf16[2,2,1024,256]{3,0,1,2:T(2,128)(2,1)S(1)} all-to-all(bf16[2,2,1024,256]{3,0,1,2:T(2,128)(2,1)S(1)} %copy.23), channel_id=1, replica_groups=mesh['sp'=32,'tp'=16] {'tp'}, dimensions={2} | all-to-all | bytes 4194304 | tf_op jit(solution)/shard_map/all_to_all | solution.py:39
  148.7 0.3 copy.24
  149.0 1.5 copy.25
  150.5 14.3 %all-to-all-start.1 = ((bf16[32,2,64,256]{3,2,1,0:T(8,128)(2,1)}), bf16[32,2,64,256]{3,2,1,0:T(8,128)(2,1)S(1)}, u32[]{:S(2)}, u32[]{:S(2)}) async-start(bf16[32,2,64,256]{3,2,1,0:T(8,128)(2,1)} %bitcast.82), calls=%async_computation.1 | async-start | bytes 4194304 | tf_op jit(solution)/shard_map/all_to_all | solution.py:38
  164.8 0.0 copy-done
  164.8 0.2 dynamic-slice_reduce_fusion
  165.0 98.1 %all-to-all-done.1 = bf16[32,2,64,256]{3,2,1,0:T(8,128)(2,1)S(1)} async-done(((bf16[32,2,64,256]{3,2,1,0:T(8,128)(2,1)}), bf16[32,2,64,256]{3,2,1,0:T(8,128)(2,1)S(1)}, u32[]{:S(2)}, u32[]{:S(2)}) %all-to-all-start.1) | async-done | bytes 2097184 | tf_op jit(solution)/shard_map/all_to_all | solution.py:38
  263.1 0.0 copy-start.6
  263.1 0.2 copy.30
  263.3 0.0 copy-start.1
  263.3 1.3 copy-done.1
  264.6 0.0 copy-done.6
  264.6 0.2 fusion.2
  264.9 0.2 fusion.32
  265.1 2.5 reduce-window.6
  267.6 0.1 slice_reduce_fusion
  267.7 0.0 copy-start.2
  267.7 3.2 %slice_bitcast_fusion = (bf16[1,64,8192]{2,1,0:T(8,128)(2,1)}, bf16[1,64,8192]{2,1,0:T(8,128)(2,1)}) fusion(bf16[1,2,64,8192]{3,2,1,0:T(8,128)(2,1)} %bitcast.80), kind=kLoop, calls=%fused_computation.26 | loop fusion | bytes 4194304 | tf_op jit(solution)/shard_map/squeeze | solution.py:46
  270.9 0.9 reduce-window.9
  271.8 0.1 slice.30
  271.9 0.1 broadcast.43
  272.0 0.0 copy-done.2
  272.0 1.0 fusion.17
  (5 shorter events, 0.1 us)
Async XLA Ops:
  7.2 157.6 %copy-start = (f32[2,16]{1,0:T(2,128)S(1)}, f32[2,16]{1,0:T(2,128)}, u32[]{:S(2)}) copy-start(f32[2,16]{1,0:T(2,128)} %param.13) | copy-start | bytes 388
  7.2 95.7 %copy-start.4 = (bf16[2,256,2048]{2,1,0:T(8,128)(2,1)S(1)}, bf16[2,256,2048]{2,1,0:T(8,128)(2,1)}, u32[]{:S(2)}) copy-start(bf16[2,256,2048]{2,1,0:T(8,128)(2,1)} %param.7) | copy-start | bytes 6291460
  7.2 95.7 %copy-start.5 = (f32[2048]{0:T(1024)S(1)}, f32[2048]{0:T(1024)}, u32[]{:S(2)}) copy-start(f32[2048]{0:T(1024)} %param.8) | copy-start | bytes 24580
  7.2 95.7 %all-gather.2.cloned.1.call-start = ((), (), s32[]{:S(2)}) async-start(), calls=%async_computation.2 | async-start | bytes 8912896 | tf_op jit(solution)/shard_map/all_gather | solution.py:26
  110.0 1.9 copy-start.3
  150.5 112.6 %all-to-all-start.1 = ((bf16[32,2,64,256]{3,2,1,0:T(8,128)(2,1)}), bf16[32,2,64,256]{3,2,1,0:T(8,128)(2,1)S(1)}, u32[]{:S(2)}, u32[]{:S(2)}) async-start(bf16[32,2,64,256]{3,2,1,0:T(8,128)(2,1)} %bitcast.82), calls=%async_computation.1 | async-start | bytes 4194304 | tf_op jit(solution)/shard_map/all_to_all | solution.py:38
  263.1 1.6 copy-start.6
  263.3 1.4 copy-start.1
  267.7 4.3 %copy-start.2 = (bf16[1,32,2,8,8,256]{5,4,1,3,2,0:T(8,128)(2,1)S(1)}, bf16[1,32,2,8,8,256]{5,4,1,3,2,0:T(8,128)(2,1)}, u32[]{:S(2)}) copy-start(bf16[1,32,2,8,8,256]{5,4,1,3,2,0:T(8,128)(2,1)} %copy-done.1) | copy-start | bytes 6291460
Sparse Core Ops, SparseCore 0:
  11.6 91.2 all-gather.1
where the time goes:
time: 281 us; the launch traced here: 280 us
  waiting for transfers between devices  189 us (67%)
  blocking collectives  32.2 us (11%)
  starting transfers between devices  14.3 us (5%)
  between operations  14.2 us (5%)
  local copies, waits for them, and re-layouts  11.8 us (4%)
  other arithmetic  10.1 us (4%)
  matrix products  8.41 us (3%)
    all_to_all x1, waiting for transfers between devices, local(): lax.all_to_all(lax.all_to_all(packed, 'tp', split_axis=2, concat_axis=0,...  98.1 us
    all_gather x1, waiting for transfers between devices, local(): lax.all_gather(stacked, 'tp', axis=1, tiled=True)  90.8 us
    all_to_all x1, blocking collectives, local(): lax.all_to_all(packed, 'tp', split_axis=2, concat_axis=0, tiled=True)  32.2 us
    all_to_all x1, starting transfers between devices, local(): lax.all_to_all(lax.all_to_all(packed, 'tp', split_axis=2, concat_axis=0,...  14.3 us
    dot_general x1, matrix products, local(): jnp.einsum('spd,knd->sknp', normed, lax.all_gather(stacked, 'tp', axis=1,...  7.13 us
  transfers between devices with their start and end apart: 2, of which 2 were waited for; matrix products, arithmetic and copies ran while one was open for 1% of the time, Pallas kernels for 0%

commit v1 on v0

v1 whole, which is shorter than its diff:
```python
import jax
import jax.numpy as jnp
from jax import lax
from jax.experimental import pallas as pl
from jax.experimental.pallas import tpu as pltpu
from jax.sharding import PartitionSpec as P

HEAD = 64
EPS = 1e-06
MESH = pl.DeviceIdType.MESH
Y, X, Z = 4, 4, 16
POS = 256
D = 2048

ORDER = [(0, 0), (1, 0), (3, 0), (0, 1), (0, 3), (2, 0), (0, 2),
         (1, 1), (1, 3), (3, 1), (3, 3), (2, 1), (2, 3), (1, 2), (3, 2), (2, 2)]
SLOT = {offset: slot for slot, offset in enumerate(ORDER)}
GROUPS = [(1, 5), (5, 7), (7, 11), (11, 15), (15, 16)]


def exchange(prompt, gain, kw, vw, kgain, kv, pbuf, nbuf, wbuf, sbuf, mbuf,
             lsem, ws, wr, fs, ps, pr, ms, mr, zs, zr):
    sp = lax.axis_index("sp")
    tp = lax.axis_index("tp")
    z, c = sp // 2, lax.rem(sp, 2)
    y, x = tp // X, lax.rem(tp, X)
    first = c == 0

    def plane(dy, dx):
        return lax.rem(y + dy + Y, Y) * X + lax.rem(x + dx + X, X)

    loads = [
        pltpu.make_async_copy(prompt.at[0], pbuf.at[0], lsem.at[0]),
        pltpu.make_async_copy(prompt.at[1], pbuf.at[1], lsem.at[1]),
        pltpu.make_async_copy(kw, wbuf.at[0, 0], lsem.at[2]),
        pltpu.make_async_copy(vw, wbuf.at[0, 1], lsem.at[3]),
    ]
    for load in loads:
        load.start()

    barrier = pltpu.get_barrier_semaphore()
    for dy, dx in ORDER[1:]:
        pl.semaphore_signal(barrier, inc=1, device_id=(sp, plane(dy, dx)), device_id_type=MESH)
    for step in range(1, 2 * Z):
        pl.semaphore_signal(barrier, inc=1, device_id=(lax.rem(sp + step, 2 * Z), tp), device_id_type=MESH)

    gain_row = gain[...]
    for parity in range(2):
        loads[parity].wait()

        @pl.loop(0, POS // 32)
        def _(step):
            rows = pl.ds(pl.multiple_of(step * 32, 32), 32)
            flat = pbuf[parity, rows, :].astype(jnp.float32)
            scale = lax.rsqrt(jnp.mean(flat * flat, axis=-1, keepdims=True) + EPS)
            nbuf[parity, rows, :] = (flat * scale * gain_row).astype(jnp.bfloat16)

    eye = lax.broadcasted_iota(jnp.int32, (HEAD, HEAD), 0) == lax.broadcasted_iota(jnp.int32, (HEAD, HEAD), 1)
    gain_col = jnp.sum(jnp.where(eye, kgain[...], 0.0), axis=1, keepdims=True)

    def project(lo, hi):
        count = hi - lo
        weights = wbuf[lo:hi].reshape(count * 2 * HEAD, D)
        for parity in range(2):
            raw = lax.dot_general(weights, nbuf[parity], (((1,), (1,)), ((), ())),
                                  preferred_element_type=jnp.float32)
            for i in range(count):
                key = raw[i * 2 * HEAD: i * 2 * HEAD + HEAD]
                scale = lax.rsqrt(jnp.mean(key * key, axis=0, keepdims=True) + EPS)
                sbuf[lo + i, parity, 0] = (key * scale * gain_col).astype(jnp.bfloat16)
                sbuf[lo + i, parity, 1] = raw[i * 2 * HEAD + HEAD: (i + 1) * 2 * HEAD].astype(jnp.bfloat16)

    loads[2].wait()
    loads[3].wait()
    project(0, 1)
    pl.semaphore_wait(barrier, 15 + 2 * Z - 1)

    def remote(src, dst, send, recv, device):
        return pltpu.make_async_remote_copy(src_ref=src, dst_ref=dst, send_sem=send, recv_sem=recv,
                                            device_id=device, device_id_type=MESH)

    sends = []

    for i, offset in enumerate(ORDER[1:7]):
        copy = remote(wbuf.at[0, c], wbuf.at[SLOT[offset], c], ws.at[i], wr.at[SLOT[offset]],
                      (sp, plane(-offset[0], -offset[1])))
        copy.start()
        sends.append(copy)

    columns = pl.ds(pl.multiple_of(sp * POS, POS), POS)

    def onward(slot):
        dy, dx = ORDER[slot]
        owner = plane(-dy, -dx)
        source = sbuf if slot == 0 else mbuf
        for parity in range(2):
            target = owner * 2 + parity
            far = remote(source.at[slot, parity], kv.at[:, :, columns], zs.at[slot, parity], zr.at[sp], (target, tp))
            near = pltpu.make_async_copy(source.at[slot, parity], kv.at[:, :, columns], zs.at[slot, parity])

            @pl.when(target != sp)
            def _():
                far.start()

            @pl.when(target == sp)
            def _():
                near.start()

    def finish(slot):
        dy, dx = ORDER[slot]
        owner = plane(-dy, -dx)
        source = sbuf if slot == 0 else mbuf
        for parity in range(2):
            target = owner * 2 + parity
            far = remote(source.at[slot, parity], kv.at[:, :, columns], zs.at[slot, parity], zr.at[sp], (target, tp))
            near = pltpu.make_async_copy(source.at[slot, parity], kv.at[:, :, columns], zs.at[slot, parity])

            @pl.when(target != sp)
            def _():
                far.wait_send()

            @pl.when(target == sp)
            def _():
                near.wait()

    onward(0)

    partner = (z * 2 + 1 - c, tp)

    def arrive(slot):
        half = remote(wbuf.at[slot, c], wbuf.at[slot, c], ps.at[slot], wr.at[slot], partner)
        half.wait_recv()
        over = remote(wbuf.at[slot, c], wbuf.at[slot, c], ps.at[slot], pr.at[slot], partner)
        over.start()
        sends.append(over)

    def other(slot):
        remote(wbuf.at[slot, 1 - c], wbuf.at[slot, 1 - c], ps.at[slot], pr.at[slot], partner).wait_recv()

    def spread(step):
        source = jnp.where(first, SLOT[(step, 0)], SLOT[(0, step)])
        for hop in (1, 3, 2):
            slot = jnp.where(first, SLOT[(step, hop)], SLOT[(hop, step)])
            target = jnp.where(first, plane(0, -hop), plane(-hop, 0))
            index = step * 4 + hop
            copy = remote(wbuf.at[source, c], wbuf.at[slot, c], fs.at[index], wr.at[slot], (sp, target))
            copy.start()
            sends.append(copy)

    def hand(slot):
        dy, dx = ORDER[slot]
        copy = remote(sbuf.at[slot], mbuf.at[slot], ms.at[slot], mr.at[slot], (sp, plane(dy, dx)))
        copy.start()
        sends.append(copy)

    def relay(slot):
        remote(sbuf.at[slot], mbuf.at[slot], ms.at[slot], mr.at[slot], (sp, tp)).wait_recv()
        onward(slot)

    for number, (lo, hi) in enumerate(GROUPS):
        for slot in range(lo, hi):
            arrive(slot)
        if number == 0:
            spread(1)
            spread(3)
        if number == 1:
            spread(2)
        for slot in range(lo, hi):
            other(slot)
        project(lo, hi)
        for slot in range(lo, hi):
            hand(slot)
        if number > 0:
            for slot in range(*GROUPS[number - 1]):
                relay(slot)
    for slot in range(*GROUPS[-1]):
        relay(slot)

    for copy in sends:
        copy.wait_send()
    for slot in range(16):
        finish(slot)

    @pl.loop(0, 2 * Z)
    def _(p):
        @pl.when(p != sp)
        def _():
            span = kv.at[:, :, pl.ds(pl.multiple_of(p * POS, POS), POS)]
            remote(span, span, zs.at[0, 0], zr.at[p], partner).wait_recv()


def read(kv, queries, bias, keys, values, out, kbuf, vbuf, lsem, ssem):
    length = kbuf.shape[1]
    head = lax.axis_index("tp")
    load_k = pltpu.make_async_copy(kv.at[0], kbuf, lsem.at[0])
    load_v = pltpu.make_async_copy(kv.at[1], vbuf, lsem.at[1])
    load_k.start()
    load_v.start()
    load_k.wait()
    store_k = pltpu.make_async_copy(kbuf, keys.at[0], ssem.at[0])
    store_k.start()
    q = jnp.concatenate([queries[0], jnp.zeros((6, HEAD), jnp.bfloat16)], axis=0)
    scores = jnp.dot(q, kbuf[...], preferred_element_type=jnp.float32) * 0.125
    row = lax.broadcasted_iota(jnp.int32, (8, 1), 0)
    scores = scores + jnp.where(row == 0, bias[0, head], bias[1, head])
    soft = jnp.log1p(jnp.exp(-jnp.abs(scores)))
    log_break = jnp.minimum(scores, 0.0) - soft
    log_keep = jnp.minimum(-scores, 0.0) - soft
    blocks = length // 128
    stacked = jnp.concatenate([log_keep[:, b * 128:(b + 1) * 128] for b in range(blocks)], axis=0)
    r = lax.broadcasted_iota(jnp.int32, (128, 256), 0)
    col = lax.broadcasted_iota(jnp.int32, (128, 256), 1)
    tri = jnp.where((r > col) | (col >= 128), 1.0, 0.0).astype(jnp.float32)
    sums = jnp.dot(stacked, tri, preferred_element_type=jnp.float32, precision=lax.Precision.HIGHEST)
    carry = jnp.zeros((8, 128), jnp.float32)
    parts = [None] * blocks
    for b in range(blocks - 1, -1, -1):
        parts[b] = sums[b * 8:(b + 1) * 8, :128] + carry
        carry = carry + sums[b * 8:(b + 1) * 8, 128:]
    later = jnp.concatenate(parts, axis=1)
    weights = jnp.exp(log_break + later).astype(jnp.bfloat16)
    load_v.wait()
    store_v = pltpu.make_async_copy(vbuf, values.at[0], ssem.at[1])
    store_v.start()
    result = lax.dot_general(weights, vbuf[...], (((1,), (1,)), ((), ())), preferred_element_type=jnp.float32)
    out[0] = result[:2].astype(jnp.bfloat16)
    store_k.wait()
    store_v.wait()


def local(prompt, input_gain, key_weight, value_weight, key_gain, queries, score_bias):
    hbm = pl.BlockSpec(memory_space=pltpu.HBM)
    vmem = pl.BlockSpec(memory_space=pltpu.VMEM)
    length = POS * 2 * Z
    dma = pltpu.SemaphoreType.DMA
    kv = pl.pallas_call(
        exchange,
        out_shape=jax.ShapeDtypeStruct((2, HEAD, length), jnp.bfloat16),
        in_specs=[hbm, vmem, hbm, hbm, vmem],
        out_specs=hbm,
        scratch_shapes=[
            pltpu.VMEM((2, POS, D), jnp.bfloat16),
            pltpu.VMEM((2, POS, D), jnp.bfloat16),
            pltpu.VMEM((16, 2, HEAD, D), jnp.bfloat16),
            pltpu.VMEM((16, 2, 2, HEAD, POS), jnp.bfloat16),
            pltpu.VMEM((16, 2, 2, HEAD, POS), jnp.bfloat16),
            dma((4,)), dma((6,)), dma((16,)), dma((16,)), dma((16,)), dma((16,)),
            dma((16,)), dma((16,)), dma((16, 2)), dma((32,)),
        ],
        compiler_params=pltpu.CompilerParams(collective_id=0, has_side_effects=True),
        name="exchange",
    )(prompt, input_gain.reshape(1, D), key_weight, value_weight, key_gain.reshape(1, HEAD))
    keys, values, out = pl.pallas_call(
        read,
        out_shape=(
            jax.ShapeDtypeStruct((1, HEAD, length), jnp.bfloat16),
            jax.ShapeDtypeStruct((1, HEAD, length), jnp.bfloat16),
            jax.ShapeDtypeStruct((1, 2, HEAD), jnp.bfloat16),
        ),
        in_specs=[hbm, vmem, pl.BlockSpec(memory_space=pltpu.SMEM)],
        out_specs=(hbm, hbm, vmem),
        scratch_shapes=[
            pltpu.VMEM((HEAD, length), jnp.bfloat16),
            pltpu.VMEM((HEAD, length), jnp.bfloat16),
            dma((2,)), dma((2,)),
        ],
        name="read",
    )(kv, queries, score_bias)
    return keys, values, out


def solution(mesh):
    placed = (P("tp", "sp", None), P(), P("tp", None), P("tp", None), P(), P("sp", None, "tp"), P())
    return jax.shard_map(
        local,
        mesh=mesh,
        in_specs=placed,
        out_specs=(P("sp", "tp", None), P("sp", "tp", None), P("sp", None, "tp")),
        check_vma=False,
    )
```

time: 281 us -> 151 us (0.54)
  the two profiles are of different devices: /device:TPU:1 before, /device:TPU:81 now
where the time goes in v1:
time: 151 us
  Pallas kernels  150 us (99%)
    pallas_call x1, Pallas kernels, local(): pl.pallas_call(exchange, out_shape=jax.ShapeDtypeStruct((2, HEAD, length)...  146 us
    pallas_call x1, Pallas kernels, local(): pl.pallas_call(read, out_shape=(jax.ShapeDtypeStruct((1, HEAD, length), j...  4.56 us

profile of v1, /device:TPU:81, one launch (start us, length us, event | category | flops | bytes accessed | tf_op | source)
XLA Modules:
  0.0 150.7 jit_solution(15901135037644057247)
XLA Ops:
  0.6 145.5 %exchange.1.kv = bf16[2,64,8192]{2,1,0:T(8,128)(2,1)} custom-call(bf16[2,256,2048]{2,1,0:T(8,128)(2,1)} %prompt.1, f32[1,2048]{1,0:T(1,128)} %bitcast.2, bf16[64,2048]{1,0:T(8,128)(2,1)} %kw.1, bf16[64,2048]{1,0:T(8,128)(2,1)} %vw.1, f32[1,64]{1,0:T(1,128)} %bitcast.3), custom_call_target="tpu_custom_call" | custom-call | tf_op jit(solution)/shard_map/exchange/pallas_call | solution.py:236
  146.2 4.6 %read.1 = (bf16[1,64,8192]{2,1,0:T(8,128)(2,1)}, bf16[1,64,8192]{2,1,0:T(8,128)(2,1)}, bf16[1,2,64]{2,1,0:T(2,128)(2,1)}) custom-call(bf16[2,64,8192]{2,1,0:T(8,128)(2,1)} %exchange.1.kv, bf16[1,2,64]{2,1,0:T(2,128)(2,1)} %queries.1, f32[2,16]{1,0:T(2,128)} %bias.1), custom_call_target="tpu_custom_call" | custom-call | tf_op jit(solution)/shard_map/read/pallas_call | solution.py:253

commit v2 on v1

--- a/solution.py
+++ b/solution.py
@@ -15,19 +15,26 @@
 ORDER = [(0, 0), (1, 0), (3, 0), (0, 1), (0, 3), (2, 0), (0, 2),
          (1, 1), (1, 3), (3, 1), (3, 3), (2, 1), (2, 3), (1, 2), (3, 2), (2, 2)]
 SLOT = {offset: slot for slot, offset in enumerate(ORDER)}
+UNIT = 16
+STEPS = [8, 7, -7, 6, -6, 5, -5, 4, -4, 3, -3, 2, -2, 1, -1, 0]
 GROUPS = [(1, 5), (5, 7), (7, 11), (11, 15), (15, 16)]
 
 
-def exchange(prompt, gain, kw, vw, kgain, kv, pbuf, nbuf, wbuf, sbuf, mbuf,
-             lsem, ws, wr, fs, ps, pr, ms, mr, zs, zr):
+def exchange(prompt, gain, kw, vw, kgain, kv, pbuf, nbuf, ubuf, xbuf, wbuf, sbuf, mbuf, ybuf, tbuf, kvbuf,
+             lsem, us, ur, bs, br, ws, wr, fs, ps, pr, ms, mr, zs, zr, ys, yr):
     sp = lax.axis_index("sp")
     tp = lax.axis_index("tp")
     z, c = sp // 2, lax.rem(sp, 2)
     y, x = tp // X, lax.rem(tp, X)
     first = c == 0
+    partner = (z * 2 + 1 - c, tp)
 
     def plane(dy, dx):
         return lax.rem(y + dy + Y, Y) * X + lax.rem(x + dx + X, X)
+
+    def remote(src, dst, send, recv, device):
+        return pltpu.make_async_remote_copy(src_ref=src, dst_ref=dst, send_sem=send, recv_sem=recv,
+                                            device_id=device, device_id_type=MESH)
 
     loads = [
         pltpu.make_async_copy(prompt.at[0], pbuf.at[0], lsem.at[0]),
@@ -45,7 +52,8 @@
         pl.semaphore_signal(barrier, inc=1, device_id=(lax.rem(sp + step, 2 * Z), tp), device_id_type=MESH)
 
     gain_row = gain[...]
-    for parity in range(2):
+
+    def norm(parity):
         loads[parity].wait()
 
         @pl.loop(0, POS // 32)
@@ -55,31 +63,23 @@
             scale = lax.rsqrt(jnp.mean(flat * flat, axis=-1, keepdims=True) + EPS)
             nbuf[parity, rows, :] = (flat * scale * gain_row).astype(jnp.bfloat16)
 
-    eye = lax.broadcasted_iota(jnp.int32, (HEAD, HEAD), 0) == lax.broadcasted_iota(jnp.int32, (HEAD, HEAD), 1)
-    gain_col = jnp.sum(jnp.where(eye, kgain[...], 0.0), axis=1, keepdims=True)
-
-    def project(lo, hi):
-        count = hi - lo
-        weights = wbuf[lo:hi].reshape(count * 2 * HEAD, D)
-        for parity in range(2):
-            raw = lax.dot_general(weights, nbuf[parity], (((1,), (1,)), ((), ())),
-                                  preferred_element_type=jnp.float32)
-            for i in range(count):
-                key = raw[i * 2 * HEAD: i * 2 * HEAD + HEAD]
-                scale = lax.rsqrt(jnp.mean(key * key, axis=0, keepdims=True) + EPS)
-                sbuf[lo + i, parity, 0] = (key * scale * gain_col).astype(jnp.bfloat16)
-                sbuf[lo + i, parity, 1] = raw[i * 2 * HEAD + HEAD: (i + 1) * 2 * HEAD].astype(jnp.bfloat16)
-
+    norm(0)
     loads[2].wait()
     loads[3].wait()
-    project(0, 1)
     pl.semaphore_wait(barrier, 15 + 2 * Z - 1)
 
-    def remote(src, dst, send, recv, device):
-        return pltpu.make_async_remote_copy(src_ref=src, dst_ref=dst, send_sem=send, recv_sem=recv,
-                                            device_id=device, device_id_type=MESH)
-
     sends = []
+
+    def unit(j):
+        return nbuf.at[0, pl.ds(pl.multiple_of(j * UNIT, UNIT), UNIT), :]
+
+    own = pltpu.make_async_copy(unit(tp), ubuf.at[tp], ur.at[tp])
+    own.start()
+    for slot, (dy, dx) in enumerate(ORDER[1:]):
+        j = plane(dy, dx)
+        copy = remote(unit(j), ubuf.at[tp], us.at[slot], ur.at[tp], (sp, j))
+        copy.start()
+        sends.append(copy)
 
     for i, offset in enumerate(ORDER[1:7]):
         copy = remote(wbuf.at[0, c], wbuf.at[SLOT[offset], c], ws.at[i], wr.at[SLOT[offset]],
@@ -87,45 +87,33 @@
         copy.start()
         sends.append(copy)
 
-    columns = pl.ds(pl.multiple_of(sp * POS, POS), POS)
-
-    def onward(slot):
-        dy, dx = ORDER[slot]
-        owner = plane(-dy, -dx)
-        source = sbuf if slot == 0 else mbuf
-        for parity in range(2):
-            target = owner * 2 + parity
-            far = remote(source.at[slot, parity], kv.at[:, :, columns], zs.at[slot, parity], zr.at[sp], (target, tp))
-            near = pltpu.make_async_copy(source.at[slot, parity], kv.at[:, :, columns], zs.at[slot, parity])
-
-            @pl.when(target != sp)
-            def _():
-                far.start()
-
-            @pl.when(target == sp)
-            def _():
-                near.start()
-
-    def finish(slot):
-        dy, dx = ORDER[slot]
-        owner = plane(-dy, -dx)
-        source = sbuf if slot == 0 else mbuf
-        for parity in range(2):
-            target = owner * 2 + parity
-            far = remote(source.at[slot, parity], kv.at[:, :, columns], zs.at[slot, parity], zr.at[sp], (target, tp))
-            near = pltpu.make_async_copy(source.at[slot, parity], kv.at[:, :, columns], zs.at[slot, parity])
-
-            @pl.when(target != sp)
-            def _():
-                far.wait_send()
-
-            @pl.when(target == sp)
-            def _():
-                near.wait()
-
-    onward(0)
-
-    partner = (z * 2 + 1 - c, tp)
+    norm(1)
+
+    rows_here = xbuf.at[pl.ds(pl.multiple_of(z * UNIT, UNIT), UNIT), :]
+    local_unit = None
+    for i, d in enumerate(STEPS):
+        t = lax.rem(z + d + Z, Z)
+        pltpu.make_async_copy(ubuf.at[t], ubuf.at[t], ur.at[t]).wait()
+        if d == 0:
+            local_unit = pltpu.make_async_copy(ubuf.at[t], rows_here, bs.at[i])
+            local_unit.start()
+        else:
+            copy = remote(ubuf.at[t], rows_here, bs.at[i], br.at[z], (t * 2 + c, tp))
+            copy.start()
+            sends.append(copy)
+
+    eye = lax.broadcasted_iota(jnp.int32, (HEAD, HEAD), 0) == lax.broadcasted_iota(jnp.int32, (HEAD, HEAD), 1)
+    gain_col = jnp.sum(jnp.where(eye, kgain[...], 0.0), axis=1, keepdims=True)
+
+    def project(lo, hi):
+        count = hi - lo
+        weights = wbuf[lo:hi].reshape(count * 2 * HEAD, D)
+        raw = lax.dot_general(weights, nbuf[1], (((1,), (1,)), ((), ())), preferred_element_type=jnp.float32)
+        for i in range(count):
+            key = raw[i * 2 * HEAD: i * 2 * HEAD + HEAD]
+            scale = lax.rsqrt(jnp.mean(key * key, axis=0, keepdims=True) + EPS)
+            sbuf[lo + i, 0] = (key * scale * gain_col).astype(jnp.bfloat16)
+            sbuf[lo + i, 1] = raw[i * 2 * HEAD + HEAD: (i + 1) * 2 * HEAD].astype(jnp.bfloat16)
 
     def arrive(slot):
         half = remote(wbuf.at[slot, c], wbuf.at[slot, c], ps.at[slot], wr.at[slot], partner)
@@ -142,21 +130,21 @@
         for hop in (1, 3, 2):
             slot = jnp.where(first, SLOT[(step, hop)], SLOT[(hop, step)])
             target = jnp.where(first, plane(0, -hop), plane(-hop, 0))
-            index = step * 4 + hop
-            copy = remote(wbuf.at[source, c], wbuf.at[slot, c], fs.at[index], wr.at[slot], (sp, target))
+            copy = remote(wbuf.at[source, c], wbuf.at[slot, c], fs.at[step * 4 + hop], wr.at[slot], (sp, target))
             copy.start()
             sends.append(copy)
 
     def hand(slot):
         dy, dx = ORDER[slot]
-        copy = remote(sbuf.at[slot], mbuf.at[slot], ms.at[slot], mr.at[slot], (sp, plane(dy, dx)))
-        copy.start()
-        sends.append(copy)
-
-    def relay(slot):
-        remote(sbuf.at[slot], mbuf.at[slot], ms.at[slot], mr.at[slot], (sp, tp)).wait_recv()
-        onward(slot)
-
+        if slot == 0:
+            pltpu.make_async_copy(sbuf.at[slot], mbuf.at[tp], mr.at[tp]).start()
+        else:
+            copy = remote(sbuf.at[slot], mbuf.at[tp], ms.at[slot], mr.at[tp], (sp, plane(dy, dx)))
+            copy.start()
+            sends.append(copy)
+
+    project(0, 1)
+    hand(0)
     for number, (lo, hi) in enumerate(GROUPS):
         for slot in range(lo, hi):
             arrive(slot)
@@ -170,23 +158,101 @@
         project(lo, hi)
         for slot in range(lo, hi):
             hand(slot)
-        if number > 0:
-            for slot in range(*GROUPS[number - 1]):
-                relay(slot)
-    for slot in range(*GROUPS[-1]):
-        relay(slot)
+
+    columns = kv.at[:, :, pl.ds(pl.multiple_of(sp * POS, POS), POS)]
+    for i, d in enumerate(STEPS):
+        t = lax.rem(z + d + Z, Z)
+        pltpu.make_async_copy(mbuf.at[t], mbuf.at[t], mr.at[t]).wait()
+        far = remote(mbuf.at[t], columns, zs.at[i], zr.at[sp], (t * 2 + 1, tp))
+        if d == 0:
+            near = pltpu.make_async_copy(mbuf.at[t], columns, zs.at[i])
+
+            @pl.when(first)
+            def _():
+                far.start()
+
+            @pl.when(jnp.logical_not(first))
+            def _():
+                near.start()
+        else:
+            far.start()
+            sends.append(far)
+
+    local_unit.wait()
+    for d in STEPS:
+        if d != 0:
+            s = lax.rem(z + d + Z, Z)
+            came = xbuf.at[pl.ds(pl.multiple_of(s * UNIT, UNIT), UNIT), :]
+            remote(came, came, bs.at[0], br.at[s], partner).wait_recv()
+
+    lane = lax.broadcasted_iota(jnp.int32, (1, 2 * HEAD), 1)
+    gain_both = jnp.concatenate([kgain[...], kgain[...]], axis=1)
+    place = tbuf.at[:, c, tp]
+    for slot, (dy, dx) in enumerate(ORDER):
+        weights = wbuf[slot].reshape(2 * HEAD, D)
+        raw = lax.dot_general(xbuf[...], weights, (((1,), (1,)), ((), ())), preferred_element_type=jnp.float32)
+        mean = jnp.sum(jnp.where(lane < HEAD, raw * raw, 0.0), axis=1, keepdims=True) * (1.0 / HEAD)
+        scale = jnp.where(lane < HEAD, lax.rsqrt(mean + EPS) * gain_both, 1.0)
+        ybuf[slot] = (raw * scale).astype(jnp.bfloat16).reshape(Z, UNIT, 2 * HEAD)
+        far = remote(ybuf.at[slot], place, ys.at[slot], yr.at[tp * 2 + c], (z * 2, plane(dy, dx)))
+        if slot == 0:
+            near_y = pltpu.make_async_copy(ybuf.at[slot], place, ys.at[slot])
+            far_y = far
+
+            @pl.when(first)
+            def _():
+                near_y.start()
+
+            @pl.when(jnp.logical_not(first))
+            def _():
+                far_y.start()
+        else:
+            far.start()
+            sends.append(far)
+
+    @pl.when(first)
+    def _():
+        near_y.wait()
+
+        @pl.loop(0, 2 * 16)
+        def _(source):
+            @pl.when(source != tp * 2)
+            def _():
+                came = tbuf.at[:, lax.rem(source, 2), source // 2]
+                remote(came, came, ys.at[0], yr.at[source], partner).wait_recv()
+
+        one = lax.broadcasted_iota(jnp.int32, (128, 128), 0) == lax.broadcasted_iota(jnp.int32, (128, 128), 1)
+        identity = jnp.where(one, 1.0, 0.0).astype(jnp.bfloat16)
+
+        @pl.loop(0, 2 * Z)
+        def _(p):
+            rows = tbuf[p // 2, lax.rem(p, 2)].reshape(POS, 2 * HEAD)
+            turned = lax.dot_general(identity, rows, (((1,), (1,)), ((), ())), preferred_element_type=jnp.float32)
+            turned = turned.astype(jnp.bfloat16)
+            span = pl.ds(pl.multiple_of(p * POS, POS), POS)
+            kvbuf[0, :, span] = turned[:HEAD]
+            kvbuf[1, :, span] = turned[HEAD:]
+
+        out = pltpu.make_async_copy(kvbuf, kv, lsem.at[0])
+        out.start()
+        out.wait()
+        far_d0 = remote(mbuf.at[z], columns, zs.at[STEPS.index(0)], zr.at[sp], (z * 2 + 1, tp))
+        far_d0.wait_send()
+
+    @pl.when(jnp.logical_not(first))
+    def _():
+        far_y.wait_send()
+        pltpu.make_async_copy(mbuf.at[z], columns, zs.at[STEPS.index(0)]).wait()
+
+        @pl.loop(0, 2 * Z)
+        def _(p):
+            @pl.when(p != sp)
+            def _():
+                span = kv.at[:, :, pl.ds(pl.multiple_of(p * POS, POS), POS)]
+                remote(span, span, zs.at[0], zr.at[p], partner).wait_recv()
 
     for copy in sends:
         copy.wait_send()
-    for slot in range(16):
-        finish(slot)
-
-    @pl.loop(0, 2 * Z)
-    def _(p):
-        @pl.when(p != sp)
-        def _():
-            span = kv.at[:, :, pl.ds(pl.multiple_of(p * POS, POS), POS)]
-            remote(span, span, zs.at[0, 0], zr.at[p], partner).wait_recv()
 
 
 def read(kv, queries, bias, keys, values, out, kbuf, vbuf, lsem, ssem):
@@ -233,19 +299,25 @@
     vmem = pl.BlockSpec(memory_space=pltpu.VMEM)
     length = POS * 2 * Z
     dma = pltpu.SemaphoreType.DMA
+    bf16 = jnp.bfloat16
     kv = pl.pallas_call(
         exchange,
         out_shape=jax.ShapeDtypeStruct((2, HEAD, length), jnp.bfloat16),
         in_specs=[hbm, vmem, hbm, hbm, vmem],
         out_specs=hbm,
         scratch_shapes=[
-            pltpu.VMEM((2, POS, D), jnp.bfloat16),
-            pltpu.VMEM((2, POS, D), jnp.bfloat16),
-            pltpu.VMEM((16, 2, HEAD, D), jnp.bfloat16),
-            pltpu.VMEM((16, 2, 2, HEAD, POS), jnp.bfloat16),
-            pltpu.VMEM((16, 2, 2, HEAD, POS), jnp.bfloat16),
-            dma((4,)), dma((6,)), dma((16,)), dma((16,)), dma((16,)), dma((16,)),
-            dma((16,)), dma((16,)), dma((16, 2)), dma((32,)),
+            pltpu.VMEM((2, POS, D), bf16),
+            pltpu.VMEM((2, POS, D), bf16),
+            pltpu.VMEM((16, UNIT, D), bf16),
+            pltpu.VMEM((Z * UNIT, D), bf16),
+            pltpu.VMEM((16, 2, HEAD, D), bf16),
+            pltpu.VMEM((16, 2, HEAD, POS), bf16),
+            pltpu.VMEM((16, 2, HEAD, POS), bf16),
+            pltpu.VMEM((16, Z, UNIT, 2 * HEAD), bf16),
+            pltpu.VMEM((Z, 2, 16, UNIT, 2 * HEAD), bf16),
+            pltpu.VMEM((2, HEAD, length), bf16),
+            dma((4,)), dma((15,)), dma((16,)), dma((16,)), dma((16,)), dma((6,)), dma((16,)), dma((16,)),
+            dma((16,)), dma((16,)), dma((16,)), dma((16,)), dma((16,)), dma((32,)), dma((16,)), dma((32,)),
         ],
         compiler_params=pltpu.CompilerParams(collective_id=0, has_side_effects=True),
         name="exchange",

time: 151 us -> 129 us (0.85)
  the two profiles are of different devices: /device:TPU:81 before, /device:TPU:1 now
where the time goes in v2:
time: 129 us
  Pallas kernels  129 us (100%)
    pallas_call x1, Pallas kernels, local(): pl.pallas_call(exchange, out_shape=jax.ShapeDtypeStruct((2, HEAD, length)...  124 us
    pallas_call x1, Pallas kernels, local(): pl.pallas_call(read, out_shape=(jax.ShapeDtypeStruct((1, HEAD, length), j...  4.56 us

profile of v2, /device:TPU:1, one launch (start us, length us, event | category | flops | bytes accessed | tf_op | source)
XLA Modules:
  0.0 129.2 jit_solution(7842226428753718946)
XLA Ops:
  0.6 124.0 %exchange.1.kv = bf16[2,64,8192]{2,1,0:T(8,128)(2,1)} custom-call(bf16[2,256,2048]{2,1,0:T(8,128)(2,1)} %prompt.1, f32[1,2048]{1,0:T(1,128)} %bitcast.2, bf16[64,2048]{1,0:T(8,128)(2,1)} %kw.1, bf16[64,2048]{1,0:T(8,128)(2,1)} %vw.1, f32[1,64]{1,0:T(1,128)} %bitcast.3), custom_call_target="tpu_custom_call" | custom-call | tf_op jit(solution)/shard_map/exchange/pallas_call | solution.py:303
  124.6 4.6 %read.1 = (bf16[1,64,8192]{2,1,0:T(8,128)(2,1)}, bf16[1,64,8192]{2,1,0:T(8,128)(2,1)}, bf16[1,2,64]{2,1,0:T(2,128)(2,1)}) custom-call(bf16[2,64,8192]{2,1,0:T(8,128)(2,1)} %exchange.1.kv, bf16[1,2,64]{2,1,0:T(2,128)(2,1)} %queries.1, f32[2,16]{1,0:T(2,128)} %bias.1), custom_call_target="tpu_custom_call" | custom-call | tf_op jit(solution)/shard_map/read/pallas_call | solution.py:325

commit v3 on v2

--- a/solution.py
+++ b/solution.py
@@ -21,7 +21,7 @@
 
 
 def exchange(prompt, gain, kw, vw, kgain, kv, pbuf, nbuf, ubuf, xbuf, wbuf, sbuf, mbuf, ybuf, tbuf, kvbuf,
-             lsem, us, ur, bs, br, ws, wr, fs, ps, pr, ms, mr, zs, zr, ys, yr):
+             tok, lsem, us, ur, bs, br, ws, wr, fs, ps, pr, ms, mr, zs, zr, ys, yr):
     sp = lax.axis_index("sp")
     tp = lax.axis_index("tp")
     z, c = sp // 2, lax.rem(sp, 2)
@@ -37,10 +37,9 @@
                                             device_id=device, device_id_type=MESH)
 
     loads = [
-        pltpu.make_async_copy(prompt.at[0], pbuf.at[0], lsem.at[0]),
-        pltpu.make_async_copy(prompt.at[1], pbuf.at[1], lsem.at[1]),
-        pltpu.make_async_copy(kw, wbuf.at[0, 0], lsem.at[2]),
-        pltpu.make_async_copy(vw, wbuf.at[0, 1], lsem.at[3]),
+        pltpu.make_async_copy(prompt.at[1], pbuf, lsem.at[0]),
+        pltpu.make_async_copy(kw, wbuf.at[0, 0], lsem.at[1]),
+        pltpu.make_async_copy(vw, wbuf.at[0, 1], lsem.at[2]),
     ]
     for load in loads:
         load.start()
@@ -48,30 +47,27 @@
     barrier = pltpu.get_barrier_semaphore()
     for dy, dx in ORDER[1:]:
         pl.semaphore_signal(barrier, inc=1, device_id=(sp, plane(dy, dx)), device_id_type=MESH)
-    for step in range(1, 2 * Z):
-        pl.semaphore_signal(barrier, inc=1, device_id=(lax.rem(sp + step, 2 * Z), tp), device_id_type=MESH)
+    ahead = (lax.rem(sp + 2, 2 * Z), tp)
+    behind = (lax.rem(sp + 2 * Z - 2, 2 * Z), tp)
+    for device in (partner, ahead, behind):
+        pl.semaphore_signal(barrier, inc=1, device_id=device, device_id_type=MESH)
 
     gain_row = gain[...]
 
-    def norm(parity):
-        loads[parity].wait()
-
+    def norm(source, target):
         @pl.loop(0, POS // 32)
         def _(step):
             rows = pl.ds(pl.multiple_of(step * 32, 32), 32)
-            flat = pbuf[parity, rows, :].astype(jnp.float32)
+            flat = source[rows, :].astype(jnp.float32)
             scale = lax.rsqrt(jnp.mean(flat * flat, axis=-1, keepdims=True) + EPS)
-            nbuf[parity, rows, :] = (flat * scale * gain_row).astype(jnp.bfloat16)
-
-    norm(0)
-    loads[2].wait()
-    loads[3].wait()
-    pl.semaphore_wait(barrier, 15 + 2 * Z - 1)
+            target[rows, :] = (flat * scale * gain_row).astype(jnp.bfloat16)
+
+    pl.semaphore_wait(barrier, 15 + 3)
 
     sends = []
 
     def unit(j):
-        return nbuf.at[0, pl.ds(pl.multiple_of(j * UNIT, UNIT), UNIT), :]
+        return prompt.at[0, pl.ds(pl.multiple_of(j * UNIT, UNIT), UNIT), :]
 
     own = pltpu.make_async_copy(unit(tp), ubuf.at[tp], ur.at[tp])
     own.start()
@@ -81,16 +77,22 @@
         copy.start()
         sends.append(copy)
 
+    loads[1].wait()
+    loads[2].wait()
     for i, offset in enumerate(ORDER[1:7]):
         copy = remote(wbuf.at[0, c], wbuf.at[SLOT[offset], c], ws.at[i], wr.at[SLOT[offset]],
                       (sp, plane(-offset[0], -offset[1])))
         copy.start()
         sends.append(copy)
 
-    norm(1)
-
     rows_here = xbuf.at[pl.ds(pl.multiple_of(z * UNIT, UNIT), UNIT), :]
     local_unit = None
+    for i, hop in enumerate((1, 2, 4)):
+        for side, d in enumerate((hop, -hop)):
+            pl.semaphore_signal(tok.at[i, side], inc=1, device_id=(lax.rem(sp + 2 * d + 2 * Z, 2 * Z), tp),
+                                device_id_type=MESH)
+        for side in range(2):
+            pl.semaphore_wait(tok.at[i, side], 1)
     for i, d in enumerate(STEPS):
         t = lax.rem(z + d + Z, Z)
         pltpu.make_async_copy(ubuf.at[t], ubuf.at[t], ur.at[t]).wait()
@@ -102,13 +104,16 @@
             copy.start()
             sends.append(copy)
 
+    loads[0].wait()
+    norm(pbuf, nbuf)
+
     eye = lax.broadcasted_iota(jnp.int32, (HEAD, HEAD), 0) == lax.broadcasted_iota(jnp.int32, (HEAD, HEAD), 1)
     gain_col = jnp.sum(jnp.where(eye, kgain[...], 0.0), axis=1, keepdims=True)
 
     def project(lo, hi):
         count = hi - lo
         weights = wbuf[lo:hi].reshape(count * 2 * HEAD, D)
-        raw = lax.dot_general(weights, nbuf[1], (((1,), (1,)), ((), ())), preferred_element_type=jnp.float32)
+        raw = lax.dot_general(weights, nbuf[...], (((1,), (1,)), ((), ())), preferred_element_type=jnp.float32)
         for i in range(count):
             key = raw[i * 2 * HEAD: i * 2 * HEAD + HEAD]
             scale = lax.rsqrt(jnp.mean(key * key, axis=0, keepdims=True) + EPS)
@@ -185,6 +190,7 @@
             came = xbuf.at[pl.ds(pl.multiple_of(s * UNIT, UNIT), UNIT), :]
             remote(came, came, bs.at[0], br.at[s], partner).wait_recv()
 
+    norm(xbuf, xbuf)
     lane = lax.broadcasted_iota(jnp.int32, (1, 2 * HEAD), 1)
     gain_both = jnp.concatenate([kgain[...], kgain[...]], axis=1)
     place = tbuf.at[:, c, tp]
@@ -306,8 +312,8 @@
         in_specs=[hbm, vmem, hbm, hbm, vmem],
         out_specs=hbm,
         scratch_shapes=[
-            pltpu.VMEM((2, POS, D), bf16),
-            pltpu.VMEM((2, POS, D), bf16),
+            pltpu.VMEM((POS, D), bf16),
+            pltpu.VMEM((POS, D), bf16),
             pltpu.VMEM((16, UNIT, D), bf16),
             pltpu.VMEM((Z * UNIT, D), bf16),
             pltpu.VMEM((16, 2, HEAD, D), bf16),
@@ -316,7 +322,7 @@
             pltpu.VMEM((16, Z, UNIT, 2 * HEAD), bf16),
             pltpu.VMEM((Z, 2, 16, UNIT, 2 * HEAD), bf16),
             pltpu.VMEM((2, HEAD, length), bf16),
-            dma((4,)), dma((15,)), dma((16,)), dma((16,)), dma((16,)), dma((6,)), dma((16,)), dma((16,)),
+            pltpu.SemaphoreType.REGULAR((8, 2)), dma((3,)), dma((15,)), dma((16,)), dma((16,)), dma((16,)), dma((6,)), dma((16,)), dma((16,)),
             dma((16,)), dma((16,)), dma((16,)), dma((16,)), dma((16,)), dma((32,)), dma((16,)), dma((32,)),
         ],
         compiler_params=pltpu.CompilerParams(collective_id=0, has_side_effects=True),

time: 129 us -> 124 us (0.961); the launches traced: 129 us -> 123 us
  Pallas kernels: 129 us -> 122 us
    pallas_call x1, Pallas kernels: 124 us -> 117 us  [local(): pl.pallas_call(exchange, out_shape=jax.ShapeDtypeStruct((2, HEAD, length)...]
where the time goes in v3:
time: 124 us; the launch traced here: 123 us
  Pallas kernels  122 us (98%)
    pallas_call x1, Pallas kernels, local(): pl.pallas_call(exchange, out_shape=jax.ShapeDtypeStruct((2, HEAD, length)...  117 us
    pallas_call x1, Pallas kernels, local(): pl.pallas_call(read, out_shape=(jax.ShapeDtypeStruct((1, HEAD, length), j...  4.56 us

profile of v3, /device:TPU:1, one launch (start us, length us, event | category | flops | bytes accessed | tf_op | source)
XLA Modules:
  0.0 122.6 jit_solution(9242034295463878599)
XLA Ops:
  0.6 117.4 %exchange.1.kv = bf16[2,64,8192]{2,1,0:T(8,128)(2,1)} custom-call(bf16[2,256,2048]{2,1,0:T(8,128)(2,1)} %prompt.1, f32[1,2048]{1,0:T(1,128)} %bitcast.2, bf16[64,2048]{1,0:T(8,128)(2,1)} %kw.1, bf16[64,2048]{1,0:T(8,128)(2,1)} %vw.1, f32[1,64]{1,0:T(1,128)} %bitcast.3), custom_call_target="tpu_custom_call" | custom-call | tf_op jit(solution)/shard_map/exchange/pallas_call | solution.py:309
  118.0 4.6 %read.1 = (bf16[1,64,8192]{2,1,0:T(8,128)(2,1)}, bf16[1,64,8192]{2,1,0:T(8,128)(2,1)}, bf16[1,2,64]{2,1,0:T(2,128)(2,1)}) custom-call(bf16[2,64,8192]{2,1,0:T(8,128)(2,1)} %exchange.1.kv, bf16[1,2,64]{2,1,0:T(2,128)(2,1)} %queries.1, f32[2,16]{1,0:T(2,128)} %bias.1), custom_call_target="tpu_custom_call" | custom-call | tf_op jit(solution)/shard_map/read/pallas_call | solution.py:331

commit v4 on v3

--- a/solution.py
+++ b/solution.py
@@ -17,10 +17,11 @@
 SLOT = {offset: slot for slot, offset in enumerate(ORDER)}
 UNIT = 16
 STEPS = [8, 7, -7, 6, -6, 5, -5, 4, -4, 3, -3, 2, -2, 1, -1, 0]
+LATER = [0, 8, 7, -7, 6, -6, 5, -5, 4, -4, 3, -3, 2, -2, 1, -1]
 GROUPS = [(1, 5), (5, 7), (7, 11), (11, 15), (15, 16)]
 
 
-def exchange(prompt, gain, kw, vw, kgain, kv, pbuf, nbuf, ubuf, xbuf, wbuf, sbuf, mbuf, ybuf, tbuf, kvbuf,
+def exchange(prompt, gain, kw, vw, kgain, queries, bias, kv, result, pbuf, nbuf, ubuf, xbuf, wbuf, sbuf, mbuf, ybuf, tbuf, parts, totals,
              tok, lsem, us, ur, bs, br, ws, wr, fs, ps, pr, ms, mr, zs, zr, ys, yr):
     sp = lax.axis_index("sp")
     tp = lax.axis_index("tp")
@@ -165,7 +166,7 @@
             hand(slot)
 
     columns = kv.at[:, :, pl.ds(pl.multiple_of(sp * POS, POS), POS)]
-    for i, d in enumerate(STEPS):
+    for i, d in enumerate(LATER):
         t = lax.rem(z + d + Z, Z)
         pltpu.make_async_copy(mbuf.at[t], mbuf.at[t], mr.at[t]).wait()
         far = remote(mbuf.at[t], columns, zs.at[i], zr.at[sp], (t * 2 + 1, tp))
@@ -236,68 +237,80 @@
             turned = lax.dot_general(identity, rows, (((1,), (1,)), ((), ())), preferred_element_type=jnp.float32)
             turned = turned.astype(jnp.bfloat16)
             span = pl.ds(pl.multiple_of(p * POS, POS), POS)
-            kvbuf[0, :, span] = turned[:HEAD]
-            kvbuf[1, :, span] = turned[HEAD:]
-
-        out = pltpu.make_async_copy(kvbuf, kv, lsem.at[0])
-        out.start()
-        out.wait()
-        far_d0 = remote(mbuf.at[z], columns, zs.at[STEPS.index(0)], zr.at[sp], (z * 2 + 1, tp))
-        far_d0.wait_send()
+            kv[0, :, span] = turned[:HEAD]
+            kv[1, :, span] = turned[HEAD:]
 
     @pl.when(jnp.logical_not(first))
     def _():
         far_y.wait_send()
-        pltpu.make_async_copy(mbuf.at[z], columns, zs.at[STEPS.index(0)]).wait()
-
-        @pl.loop(0, 2 * Z)
-        def _(p):
-            @pl.when(p != sp)
-            def _():
-                span = kv.at[:, :, pl.ds(pl.multiple_of(p * POS, POS), POS)]
-                remote(span, span, zs.at[0], zr.at[p], partner).wait_recv()
-
-    for copy in sends:
-        copy.wait_send()
-
-
-def read(kv, queries, bias, keys, values, out, kbuf, vbuf, lsem, ssem):
-    length = kbuf.shape[1]
-    head = lax.axis_index("tp")
-    load_k = pltpu.make_async_copy(kv.at[0], kbuf, lsem.at[0])
-    load_v = pltpu.make_async_copy(kv.at[1], vbuf, lsem.at[1])
-    load_k.start()
-    load_v.start()
-    load_k.wait()
-    store_k = pltpu.make_async_copy(kbuf, keys.at[0], ssem.at[0])
-    store_k.start()
+        pltpu.make_async_copy(mbuf.at[z], columns, zs.at[LATER.index(0)]).wait()
+
     q = jnp.concatenate([queries[0], jnp.zeros((6, HEAD), jnp.bfloat16)], axis=0)
-    scores = jnp.dot(q, kbuf[...], preferred_element_type=jnp.float32) * 0.125
     row = lax.broadcasted_iota(jnp.int32, (8, 1), 0)
-    scores = scores + jnp.where(row == 0, bias[0, head], bias[1, head])
-    soft = jnp.log1p(jnp.exp(-jnp.abs(scores)))
-    log_break = jnp.minimum(scores, 0.0) - soft
-    log_keep = jnp.minimum(-scores, 0.0) - soft
-    blocks = length // 128
-    stacked = jnp.concatenate([log_keep[:, b * 128:(b + 1) * 128] for b in range(blocks)], axis=0)
+    offset = jnp.where(row == 0, bias[0, tp], bias[1, tp])
     r = lax.broadcasted_iota(jnp.int32, (128, 256), 0)
     col = lax.broadcasted_iota(jnp.int32, (128, 256), 1)
     tri = jnp.where((r > col) | (col >= 128), 1.0, 0.0).astype(jnp.float32)
-    sums = jnp.dot(stacked, tri, preferred_element_type=jnp.float32, precision=lax.Precision.HIGHEST)
-    carry = jnp.zeros((8, 128), jnp.float32)
-    parts = [None] * blocks
-    for b in range(blocks - 1, -1, -1):
-        parts[b] = sums[b * 8:(b + 1) * 8, :128] + carry
-        carry = carry + sums[b * 8:(b + 1) * 8, 128:]
-    later = jnp.concatenate(parts, axis=1)
-    weights = jnp.exp(log_break + later).astype(jnp.bfloat16)
-    load_v.wait()
-    store_v = pltpu.make_async_copy(vbuf, values.at[0], ssem.at[1])
-    store_v.start()
-    result = lax.dot_general(weights, vbuf[...], (((1,), (1,)), ((), ())), preferred_element_type=jnp.float32)
-    out[0] = result[:2].astype(jnp.bfloat16)
-    store_k.wait()
-    store_v.wait()
+    span = 2 * POS
+
+    @pl.loop(0, Z)
+    def _(i):
+        far_by = Z // 2 - i // 2
+        d = jnp.where(i == 0, 0, jnp.where(lax.rem(i, 2) == 0, far_by, -far_by))
+        s = lax.rem(z - d + Z, Z)
+
+        @pl.when(jnp.logical_not(first))
+        def _():
+            for core in range(2):
+                p = s * 2 + core
+
+                @pl.when(p != sp)
+                def _():
+                    came = kv.at[:, :, pl.ds(pl.multiple_of(p * POS, POS), POS)]
+                    remote(came, came, zs.at[0], zr.at[p], partner).wait_recv()
+
+        at = pl.ds(pl.multiple_of(s * span, span), span)
+        scores = jnp.dot(q, kv[0, :, at], preferred_element_type=jnp.float32) * 0.125 + offset
+        soft = jnp.log1p(jnp.exp(-jnp.abs(scores)))
+        log_break = jnp.minimum(scores, 0.0) - soft
+        log_keep = jnp.minimum(-scores, 0.0) - soft
+        stacked = jnp.concatenate([log_keep[:, b * 128:(b + 1) * 128] for b in range(span // 128)], axis=0)
+        sums = jnp.dot(stacked, tri, preferred_element_type=jnp.float32, precision=lax.Precision.HIGHEST)
+        carry = jnp.zeros((8, 128), jnp.float32)
+        pieces = [None] * (span // 128)
+        for b in range(span // 128 - 1, -1, -1):
+            pieces[b] = sums[b * 8:(b + 1) * 8, :128] + carry
+            carry = carry + sums[b * 8:(b + 1) * 8, 128:]
+        weights = jnp.exp(log_break + jnp.concatenate(pieces, axis=1))
+        high = weights.astype(jnp.bfloat16)
+        low = (weights - high.astype(jnp.float32)).astype(jnp.bfloat16)
+        both = lax.dot_general(jnp.concatenate([high, low], axis=0), kv[1, :, at], (((1,), (1,)), ((), ())),
+                               preferred_element_type=jnp.float32)
+        parts[s] = both[:8] + both[8:]
+        totals[s] = carry
+
+    later = jnp.zeros((8, HEAD), jnp.float32)
+    total = jnp.zeros((8, HEAD), jnp.float32)
+    for s in range(Z - 1, -1, -1):
+        total = total + jnp.exp(later) * parts[s]
+        later = later + totals[s, :, :HEAD]
+    result[...] = total
+
+    @pl.when(first)
+    def _():
+        remote(mbuf.at[z], columns, zs.at[LATER.index(0)], zr.at[sp], (z * 2 + 1, tp)).wait_send()
+
+    for copy in sends:
+        copy.wait_send()
+
+
+def store(kv, result, keys, values, out, sems):
+    copies = [pltpu.make_async_copy(kv.at[i], (keys, values)[i].at[0], sems.at[i]) for i in range(2)]
+    for copy in copies:
+        copy.start()
+    out[0] = result[:2, :].astype(jnp.bfloat16)
+    for copy in copies:
+        copy.wait()
 
 
 def local(prompt, input_gain, key_weight, value_weight, key_gain, queries, score_bias):
@@ -306,11 +319,11 @@
     length = POS * 2 * Z
     dma = pltpu.SemaphoreType.DMA
     bf16 = jnp.bfloat16
-    kv = pl.pallas_call(
+    kv, result = pl.pallas_call(
         exchange,
-        out_shape=jax.ShapeDtypeStruct((2, HEAD, length), jnp.bfloat16),
-        in_specs=[hbm, vmem, hbm, hbm, vmem],
-        out_specs=hbm,
+        out_shape=(pltpu.VMEM((2, HEAD, length), bf16), pltpu.VMEM((8, HEAD), jnp.float32)),
+        in_specs=[hbm, vmem, hbm, hbm, vmem, vmem, pl.BlockSpec(memory_space=pltpu.SMEM)],
+        out_specs=(vmem, vmem),
         scratch_shapes=[
             pltpu.VMEM((POS, D), bf16),
             pltpu.VMEM((POS, D), bf16),
@@ -321,29 +334,27 @@
             pltpu.VMEM((16, 2, HEAD, POS), bf16),
             pltpu.VMEM((16, Z, UNIT, 2 * HEAD), bf16),
             pltpu.VMEM((Z, 2, 16, UNIT, 2 * HEAD), bf16),
-            pltpu.VMEM((2, HEAD, length), bf16),
+            pltpu.VMEM((Z, 8, HEAD), jnp.float32),
+            pltpu.VMEM((Z, 8, 128), jnp.float32),
             pltpu.SemaphoreType.REGULAR((8, 2)), dma((3,)), dma((15,)), dma((16,)), dma((16,)), dma((16,)), dma((6,)), dma((16,)), dma((16,)),
             dma((16,)), dma((16,)), dma((16,)), dma((16,)), dma((16,)), dma((32,)), dma((16,)), dma((32,)),
         ],
         compiler_params=pltpu.CompilerParams(collective_id=0, has_side_effects=True),
         name="exchange",
-    )(prompt, input_gain.reshape(1, D), key_weight, value_weight, key_gain.reshape(1, HEAD))
+    )(prompt, input_gain.reshape(1, D), key_weight, value_weight, key_gain.reshape(1, HEAD),
+      queries, score_bias)
     keys, values, out = pl.pallas_call(
-        read,
+        store,
         out_shape=(
-            jax.ShapeDtypeStruct((1, HEAD, length), jnp.bfloat16),
-            jax.ShapeDtypeStruct((1, HEAD, length), jnp.bfloat16),
-            jax.ShapeDtypeStruct((1, 2, HEAD), jnp.bfloat16),
+            jax.ShapeDtypeStruct((1, HEAD, length), bf16),
+            jax.ShapeDtypeStruct((1, HEAD, length), bf16),
+            jax.ShapeDtypeStruct((1, 2, HEAD), bf16),
         ),
-        in_specs=[hbm, vmem, pl.BlockSpec(memory_space=pltpu.SMEM)],
+        in_specs=[vmem, vmem],
         out_specs=(hbm, hbm, vmem),
-        scratch_shapes=[
-            pltpu.VMEM((HEAD, length), jnp.bfloat16),
-            pltpu.VMEM((HEAD, length), jnp.bfloat16),
-            dma((2,)), dma((2,)),
-        ],
-        name="read",
-    )(kv, queries, score_bias)
+        scratch_shapes=[dma((2,))],
+        name="store",
+    )(pltpu.with_memory_space_constraint(kv, pltpu.VMEM), pltpu.with_memory_space_constraint(result, pltpu.VMEM))
     return keys, values, out
 
 

time: 124 us -> 123 us (level)
  Pallas kernels: 122 us -> 120 us
    pallas_call x2, Pallas kernels: 122 us -> 120 us  [the longest x1 118 us: local(): pl.pallas_call(exchange, out_shape=(pltpu.VMEM((2, HEAD, length), bf16),...]
where the time goes in v4:
time: 123 us; the launch traced here: 121 us
  Pallas kernels  120 us (98%)
    pallas_call x1, Pallas kernels, local(): pl.pallas_call(exchange, out_shape=(pltpu.VMEM((2, HEAD, length), bf16),...  118 us

profile of v4, /device:TPU:1, one launch (start us, length us, event | category | flops | bytes accessed | tf_op | source)
XLA Modules:
  0.0 120.9 jit_solution(5198696056931883420)
XLA Ops:
  0.6 118.4 %exchange.1 = (bf16[2,64,8192]{2,1,0:T(8,128)(2,1)S(1)}, f32[8,64]{1,0:T(8,128)S(1)}) custom-call(bf16[2,256,2048]{2,1,0:T(8,128)(2,1)} %prompt.1, f32[1,2048]{1,0:T(1,128)} %bitcast.2, bf16[64,2048]{1,0:T(8,128)(2,1)} %kw.1, bf16[64,2048]{1,0:T(8,128)(2,1)} %vw.1, f32[1,64]{1,0:T(1,128)} %bitcast.3, bf16[1,2,64]{2,1,0:T(2,128)(2,1)} %queries.1, f32[2,16]{1,0:T(2,128)} %bias.1), custom_call_target="tpu_custom_call" | custom-call | tf_op jit(solution)/shard_map/exchange/pallas_call | solution.py:322
  119.1 1.8 %store.1 = (bf16[1,64,8192]{2,1,0:T(8,128)(2,1)}, bf16[1,64,8192]{2,1,0:T(8,128)(2,1)}, bf16[1,2,64]{2,1,0:T(2,128)(2,1)}) custom-call(bf16[2,64,8192]{2,1,0:T(8,128)(2,1)S(1)} %get-tuple-element.5.kv, f32[8,64]{1,0:T(8,128)S(1)} %get-tuple-element.6.result), custom_call_target="tpu_custom_call" | custom-call | tf_op jit(solution)/shard_map/store/pallas_call | solution.py:346

commit v5 on v4

--- a/solution.py
+++ b/solution.py
@@ -65,7 +65,7 @@
 
     pl.semaphore_wait(barrier, 15 + 3)
 
-    sends = []
+    sends, last = [], []
 
     def unit(j):
         return prompt.at[0, pl.ds(pl.multiple_of(j * UNIT, UNIT), UNIT), :]
@@ -78,13 +78,14 @@
         copy.start()
         sends.append(copy)
 
-    loads[1].wait()
-    loads[2].wait()
-    for i, offset in enumerate(ORDER[1:7]):
-        copy = remote(wbuf.at[0, c], wbuf.at[SLOT[offset], c], ws.at[i], wr.at[SLOT[offset]],
-                      (sp, plane(-offset[0], -offset[1])))
-        copy.start()
-        sends.append(copy)
+    def send_weights():
+        loads[1].wait()
+        loads[2].wait()
+        for i, offset in enumerate(ORDER[1:7]):
+            copy = remote(wbuf.at[0, c], wbuf.at[SLOT[offset], c], ws.at[i], wr.at[SLOT[offset]],
+                          (sp, plane(-offset[0], -offset[1])))
+            copy.start()
+            sends.append(copy)
 
     rows_here = xbuf.at[pl.ds(pl.multiple_of(z * UNIT, UNIT), UNIT), :]
     local_unit = None
@@ -94,6 +95,7 @@
                                 device_id_type=MESH)
         for side in range(2):
             pl.semaphore_wait(tok.at[i, side], 1)
+    send_weights()
     for i, d in enumerate(STEPS):
         t = lax.rem(z + d + Z, Z)
         pltpu.make_async_copy(ubuf.at[t], ubuf.at[t], ur.at[t]).wait()
@@ -182,7 +184,7 @@
                 near.start()
         else:
             far.start()
-            sends.append(far)
+            last.append(far)
 
     local_unit.wait()
     for d in STEPS:
@@ -245,12 +247,15 @@
         far_y.wait_send()
         pltpu.make_async_copy(mbuf.at[z], columns, zs.at[LATER.index(0)]).wait()
 
+    for copy in sends:
+        copy.wait_send()
+
     q = jnp.concatenate([queries[0], jnp.zeros((6, HEAD), jnp.bfloat16)], axis=0)
     row = lax.broadcasted_iota(jnp.int32, (8, 1), 0)
     offset = jnp.where(row == 0, bias[0, tp], bias[1, tp])
     r = lax.broadcasted_iota(jnp.int32, (128, 256), 0)
     col = lax.broadcasted_iota(jnp.int32, (128, 256), 1)
-    tri = jnp.where((r > col) | (col >= 128), 1.0, 0.0).astype(jnp.float32)
+    tri = jnp.where((r > col) | (col >= 128), 1.0, 0.0).astype(jnp.bfloat16)
     span = 2 * POS
 
     @pl.loop(0, Z)
@@ -275,7 +280,13 @@
         log_break = jnp.minimum(scores, 0.0) - soft
         log_keep = jnp.minimum(-scores, 0.0) - soft
         stacked = jnp.concatenate([log_keep[:, b * 128:(b + 1) * 128] for b in range(span // 128)], axis=0)
-        sums = jnp.dot(stacked, tri, preferred_element_type=jnp.float32, precision=lax.Precision.HIGHEST)
+        thirds = []
+        for _ in range(3):
+            thirds.append(stacked.astype(jnp.bfloat16))
+            stacked = stacked - thirds[-1].astype(jnp.float32)
+        rows = 8 * (span // 128)
+        sums = jnp.dot(jnp.concatenate(thirds, axis=0), tri, preferred_element_type=jnp.float32)
+        sums = (sums[2 * rows:] + sums[rows:2 * rows]) + sums[:rows]
         carry = jnp.zeros((8, 128), jnp.float32)
         pieces = [None] * (span // 128)
         for b in range(span // 128 - 1, -1, -1):
@@ -300,7 +311,7 @@
     def _():
         remote(mbuf.at[z], columns, zs.at[LATER.index(0)], zr.at[sp], (z * 2 + 1, tp)).wait_send()
 
-    for copy in sends:
+    for copy in last:
         copy.wait_send()
 
 

time: 123 us -> 121 us (0.984); the launches traced: 121 us -> 121 us
  no operation moved by 1% of the time
where the time goes in v5:
time: 121 us
  Pallas kernels  120 us (99%)
    pallas_call x1, Pallas kernels, local(): pl.pallas_call(exchange, out_shape=(pltpu.VMEM((2, HEAD, length), bf16),...  118 us

profile of v5, /device:TPU:1, one launch (start us, length us, event | category | flops | bytes accessed | tf_op | source)
XLA Modules:
  0.0 120.8 jit_solution(14359555448832914493)
XLA Ops:
  0.6 118.3 %exchange.1 = (bf16[2,64,8192]{2,1,0:T(8,128)(2,1)S(1)}, f32[8,64]{1,0:T(8,128)S(1)}) custom-call(bf16[2,256,2048]{2,1,0:T(8,128)(2,1)} %prompt.1, f32[1,2048]{1,0:T(1,128)} %bitcast.2, bf16[64,2048]{1,0:T(8,128)(2,1)} %kw.1, bf16[64,2048]{1,0:T(8,128)(2,1)} %vw.1, f32[1,64]{1,0:T(1,128)} %bitcast.3, bf16[1,2,64]{2,1,0:T(2,128)(2,1)} %queries.1, f32[2,16]{1,0:T(2,128)} %bias.1), custom_call_target="tpu_custom_call" | custom-call | tf_op jit(solution)/shard_map/exchange/pallas_call | solution.py:333
  118.9 1.8 %store.1 = (bf16[1,64,8192]{2,1,0:T(8,128)(2,1)}, bf16[1,64,8192]{2,1,0:T(8,128)(2,1)}, bf16[1,2,64]{2,1,0:T(2,128)(2,1)}) custom-call(bf16[2,64,8192]{2,1,0:T(8,128)(2,1)S(1)} %get-tuple-element.5.kv, f32[8,64]{1,0:T(8,128)S(1)} %get-tuple-element.6.result), custom_call_target="tpu_custom_call" | custom-call | tf_op jit(solution)/shard_map/store/pallas_call | solution.py:357

commit v6 on v5

--- a/solution.py
+++ b/solution.py
@@ -63,7 +63,13 @@
             scale = lax.rsqrt(jnp.mean(flat * flat, axis=-1, keepdims=True) + EPS)
             target[rows, :] = (flat * scale * gain_row).astype(jnp.bfloat16)
 
+    def tell(i, hop):
+        for side, d in enumerate((hop, -hop)):
+            pl.semaphore_signal(tok.at[i, side], inc=1, device_id=(lax.rem(sp + 2 * d + 2 * Z, 2 * Z), tp),
+                                device_id_type=MESH)
+
     pl.semaphore_wait(barrier, 15 + 3)
+    tell(0, 1)
 
     sends, last = [], []
 
@@ -90,9 +96,8 @@
     rows_here = xbuf.at[pl.ds(pl.multiple_of(z * UNIT, UNIT), UNIT), :]
     local_unit = None
     for i, hop in enumerate((1, 2, 4)):
-        for side, d in enumerate((hop, -hop)):
-            pl.semaphore_signal(tok.at[i, side], inc=1, device_id=(lax.rem(sp + 2 * d + 2 * Z, 2 * Z), tp),
-                                device_id_type=MESH)
+        if hop > 1:
+            tell(i, hop)
         for side in range(2):
             pl.semaphore_wait(tok.at[i, side], 1)
     send_weights()

time: 121 us -> 121 us (level)
  no operation moved by 1% of the time
where the time goes in v6:
time: 121 us
  Pallas kernels  120 us (99%)
    pallas_call x1, Pallas kernels, local(): pl.pallas_call(exchange, out_shape=(pltpu.VMEM((2, HEAD, length), bf16),...  118 us

profile of v6, /device:TPU:1, one launch (start us, length us, event | category | flops | bytes accessed | tf_op | source)
XLA Modules:
  0.0 120.8 jit_solution(4398843689366086146)
XLA Ops:
  0.6 118.3 %exchange.1 = (bf16[2,64,8192]{2,1,0:T(8,128)(2,1)S(1)}, f32[8,64]{1,0:T(8,128)S(1)}) custom-call(bf16[2,256,2048]{2,1,0:T(8,128)(2,1)} %prompt.1, f32[1,2048]{1,0:T(1,128)} %bitcast.2, bf16[64,2048]{1,0:T(8,128)(2,1)} %kw.1, bf16[64,2048]{1,0:T(8,128)(2,1)} %vw.1, f32[1,64]{1,0:T(1,128)} %bitcast.3, bf16[1,2,64]{2,1,0:T(2,128)(2,1)} %queries.1, f32[2,16]{1,0:T(2,128)} %bias.1), custom_call_target="tpu_custom_call" | custom-call | tf_op jit(solution)/shard_map/exchange/pallas_call | solution.py:338
  118.9 1.8 %store.1 = (bf16[1,64,8192]{2,1,0:T(8,128)(2,1)}, bf16[1,64,8192]{2,1,0:T(8,128)(2,1)}, bf16[1,2,64]{2,1,0:T(2,128)(2,1)}) custom-call(bf16[2,64,8192]{2,1,0:T(8,128)(2,1)S(1)} %get-tuple-element.5.kv, f32[8,64]{1,0:T(8,128)S(1)} %get-tuple-element.6.result), custom_call_target="tpu_custom_call" | custom-call | tf_op jit(solution)/shard_map/store/pallas_call | solution.py:362
